TPU v7x, 32 devices: a whole 2x2x4 slice. The times are simulated.
32 devices in a mesh: gr: 2 (over x), fs: 8 (over z, y), tp: 2 (over core).
Axes of the slice: x: 2, y: 2, z: 4, core: 2. Of those that a mesh axis runs over, the one named last changes fastest.
Arguments:
- tokens: bfloat16 [16384, 3072], P(('gr', 'fs')), may hold values from -6 to 6
- norm_gain: float32 [3072], P(('gr', 'fs')), may hold values from 0.1 to 1.9
- gate_weight: float32 [8, 3072, 768], P(None, ('gr', 'fs'), 'tp'), may hold values from -0.109375 to 0.109375
- up_weight: float32 [8, 3072, 768], P(None, ('gr', 'fs'), 'tp'), may hold values from -0.109375 to 0.109375
- down_weight: float32 [8, 3072, 768], P(None, ('gr', 'fs'), 'tp'), may hold values from -0.21875 to 0.21875
- group_pick: int32 [16384], P(('gr', 'fs')), may hold values from 0 to 3, as said below
- expert_pick: int32 [16384, 2], P(('gr', 'fs')), may hold values from 0 to 1, as said below
- route_weight: float32 [16384, 2], P(('gr', 'fs')), may hold values from 0.1 to 1
Outputs:
- combined: bfloat16 [16384, 3072], P(('gr', 'fs'), 'tp')
- gate_served: bfloat16 [8, 3072, 768], P('fs', None, 'tp')
- up_served: bfloat16 [8, 3072, 768], P('fs', None, 'tp')
- down_served: bfloat16 [8, 3072, 768], P('fs', None, 'tp')
Inputs may be any that keep to these rules, and one draw needn't show every extreme that they name: `group_pick`: in each aligned block of 1024 rows every group is picked by the same number of rows. `expert_pick`: the 2 entries of a row differ. In each aligned block of 1024 rows, every expert (group and number together) is named exactly 256 times.
All inputs are finite; a program needn't handle non-finite values.
Results may differ from a plain program's by a relative error of at most 0.0092.
Values may be sent and summed in bfloat16 or wider, within the bound.
A program may use at most 128 MiB of HBM per device.

v0:
```python
import jax
import jax.numpy as jnp
from jax import lax
from jax.sharding import PartitionSpec as P

GROUPS = 4


EPS = 1e-06


def local(
    tokens, norm_gain, gate_weight, up_weight, down_weight, group_pick, expert_pick, route_weight
):
    scaled = norm_gain[None, :, None]
    gate_local = (scaled * gate_weight).astype(jnp.bfloat16)
    up_local = (scaled * up_weight).astype(jnp.bfloat16)
    down_local = down_weight.astype(jnp.bfloat16)
    experts, rows_dev, cols_dev = gate_local.shape
    gate_four = gate_local.reshape(experts, 1, rows_dev, cols_dev)
    up_four = up_local.reshape(experts, 1, rows_dev, cols_dev)
    down_four = down_local.reshape(experts, 1, rows_dev, cols_dev)
    gathered = (
        lax.all_gather(gate_four, "gr", axis=1, tiled=True),
        lax.all_gather(up_four, "gr", axis=1, tiled=True),
        lax.all_gather(down_four, "gr", axis=1, tiled=True),
    )
    relaid = (
        lax.all_to_all(gathered[0], "fs", split_axis=0, concat_axis=2, tiled=True),
        lax.all_to_all(gathered[1], "fs", split_axis=0, concat_axis=2, tiled=True),
        lax.all_to_all(gathered[2], "fs", split_axis=0, concat_axis=2, tiled=True),
    )
    gate_new = relaid[0].reshape(1, -1, cols_dev)
    up_new = relaid[1].reshape(1, -1, cols_dev)
    down_new = relaid[2].reshape(1, -1, cols_dev)
    tok_rows, model_width = tokens.shape
    as_float = tokens.astype(jnp.float32)
    normed = (
        as_float * lax.rsqrt(jnp.mean(as_float * as_float, axis=-1, keepdims=True) + EPS)
    ).astype(jnp.bfloat16)
    per_group = experts // GROUPS
    top_count = expert_pick.shape[1]
    capacity = top_count * tok_rows // experts
    flat_ids = (group_pick[:, None] * per_group + expert_pick).reshape(-1)
    onehot = (flat_ids[:, None] == jnp.arange(experts, dtype=jnp.int32)[None, :]).astype(jnp.int32)
    slot_index = jnp.sum(onehot * (jnp.cumsum(onehot, axis=0) - 1), axis=1)
    target = flat_ids * capacity + slot_index
    source = (
        jnp.zeros((experts * capacity,), jnp.int32)
        .at[target]
        .set(jnp.arange(top_count * tok_rows, dtype=jnp.int32) // top_count)
    )
    outgoing = normed[source].reshape(experts, capacity, model_width)
    share = capacity // lax.axis_size("tp")
    start = lax.axis_index("tp") * share
    my_share = lax.dynamic_slice_in_dim(outgoing, start, share, 1)
    landed = lax.all_to_all(my_share, "fs", split_axis=0, concat_axis=1, tiled=True).reshape(
        experts, share, model_width
    )
    arrived = lax.all_gather(landed, "tp", axis=1, tiled=True).reshape(-1, model_width)
    gate_acts = jnp.dot(arrived, gate_new[0], preferred_element_type=jnp.float32)
    up_acts = jnp.dot(arrived, up_new[0], preferred_element_type=jnp.float32)
    hidden = (jax.nn.silu(gate_acts) * up_acts).astype(jnp.bfloat16)
    partial_value = lax.dot_general(
        hidden, down_new[0], (((1,), (1,)), ((), ())), preferred_element_type=jnp.float32
    ).astype(jnp.bfloat16)
    summed = (
        lax.psum_scatter(partial_value, "tp", scatter_dimension=1, tiled=True)
        .astype(jnp.float32)
        .astype(jnp.bfloat16)
    )
    returned = lax.all_to_all(summed, "fs", split_axis=0, concat_axis=0, tiled=True)
    picked = returned[target].reshape(tok_rows, top_count, -1).astype(jnp.float32)
    combined = jnp.sum(route_weight[:, :, None] * picked, axis=1).astype(jnp.bfloat16)
    return (combined, gate_new, up_new, down_new)


def solution(mesh):
    in_specs = (
        P(("gr", "fs"), None),
        P(("gr", "fs")),
        P(None, ("gr", "fs"), "tp"),
        P(None, ("gr", "fs"), "tp"),
        P(None, ("gr", "fs"), "tp"),
        P(("gr", "fs")),
        P(("gr", "fs"), None),
        P(("gr", "fs"), None),
    )
    out_specs = (
        P(("gr", "fs"), "tp"),
        P("fs", None, "tp"),
        P("fs", None, "tp"),
        P("fs", None, "tp"),
    )
    return jax.shard_map(local, mesh=mesh, in_specs=in_specs, out_specs=out_specs, check_vma=False)
```

profile of v0, /device:TPU:0, one launch (start us, length us, event | category | flops | bytes accessed | tf_op | source)
XLA Modules:
  0.0 640.0 jit_solution(4031025524227223699)
XLA Ops:
  12.8 8.0 %scatter_custom_fusion = s32[2048]{0:T(1024)S(1)} fusion(s32[2048]{0:T(1024)S(1)} %bitcast.62, s32[2048]{0:T(1024)S(1)} %add_select_fusion, s32[]{:T(128)} %constant.39.clone.1), kind=kCustom, calls=%fused_computation.34 | custom fusion | bytes 8196 | tf_op jit(solution)/shard_map/scatter | solution.py:51
  20.9 4.2 fusion
  25.5 5.1 fusion.1
  30.6 26.6 %gather_fusion = bf16[2048,3072]{1,0:T(8,128)(2,1)} fusion(bf16[1024,3072]{1,0:T(8,128)(2,1)} %fusion.1, s32[2048]{0:T(1024)S(1)} %fusion.8), kind=kCustom, calls=%fused_computation | custom fusion | bytes 25174016 | tf_op jit(solution)/shard_map/gather | solution.py:53
  57.2 5.9 constant_dynamic-slice_fusion
  63.1 7.4 %all-to-all-start = ((bf16[8,128,3072]{2,1,0:T(8,128)(2,1)}), bf16[8,128,3072]{2,1,0:T(8,128)(2,1)}, u32[]{:S(2)}, u32[]{:S(2)}) async-start(bf16[8,128,3072]{2,1,0:T(8,128)(2,1)} %constant_dynamic-slice_fusion), calls=%async_computation | async-start | bytes 12582912 | tf_op jit(solution)/shard_map/all_to_all | solution.py:57
  70.6 4.5 multiply_convert_fusion.1
  77.1 131.6 %all-to-all-done = bf16[8,128,3072]{2,1,0:T(8,128)(2,1)} async-done(((bf16[8,128,3072]{2,1,0:T(8,128)(2,1)}), bf16[8,128,3072]{2,1,0:T(8,128)(2,1)}, u32[]{:S(2)}, u32[]{:S(2)}) %all-to-all-start) | async-done | bytes 6291488 | tf_op jit(solution)/shard_map/all_to_all | solution.py:57
  208.8 3.6 all-to-all-start.1
  212.5 54.0 %all-to-all-done.1 = bf16[8,2,192,384]{3,2,1,0:T(8,128)(2,1)S(1)} async-done(((bf16[8,2,192,384]{3,2,1,0:T(8,128)(2,1)}), bf16[8,2,192,384]{3,2,1,0:T(8,128)(2,1)S(1)}, u32[]{:S(2)}, u32[]{:S(2)}) %all-to-all-start.1) | async-done | bytes 2359328 | tf_op jit(solution)/shard_map/all_to_all | solution.py:29
  266.5 4.4 all-to-all-start.2
  270.9 53.4 %all-to-all-done.2 = bf16[8,2,192,384]{3,2,1,0:T(8,128)(2,1)} async-done(((bf16[8,2,192,384]{3,2,1,0:T(8,128)(2,1)}), bf16[8,2,192,384]{3,2,1,0:T(8,128)(2,1)}, u32[]{:S(2)}, u32[]{:S(2)}) %all-to-all-start.2) | async-done | bytes 2359328 | tf_op jit(solution)/shard_map/all_to_all | solution.py:30
  324.3 4.4 all-to-all-start.3
  330.6 3.3 copy.32
  333.9 48.2 %all-to-all-done.3 = bf16[8,2,192,384]{3,2,1,0:T(8,128)(2,1)} async-done(((bf16[8,2,192,384]{3,2,1,0:T(8,128)(2,1)}), bf16[8,2,192,384]{3,2,1,0:T(8,128)(2,1)}, u32[]{:S(2)}, u32[]{:S(2)}) %all-to-all-start.3) | async-done | bytes 2359328 | tf_op jit(solution)/shard_map/all_to_all | solution.py:31
  382.1 3.3 copy.33
  385.4 10.7 %fusion.13 = f32[2048,384]{1,0:T(8,128)} fusion(bf16[2048,3072]{1,0:T(8,128)(2,1)} %bitcast.65, bf16[3072,384]{1,0:T(8,128)(2,1)S(1)} %bitcast.54), kind=kOutput, calls=%fused_computation.40 | convolution fusion | flops 4831838208 | bytes 18087936 | tf_op jit(solution)/shard_map/dot_general | solution.py:61
  396.1 20.7 %convolution_convert_fusion = bf16[2048,3072]{1,0:T(8,128)(2,1)} fusion(bf16[3072,384]{1,0:T(8,128)(2,1)} %bitcast.59, f32[2048,384]{1,0:T(8,128)} %fusion.13, bf16[2048,3072]{1,0:T(8,128)(2,1)} %bitcast.66, bf16[3072,384]{1,0:T(8,128)(2,1)} %bitcast.55), kind=kOutput, calls=%fused_computation.8 | convolution fusion | flops 9674686464 | bytes 33030144 | tf_op jit(solution)/shard_map/dot_general | solution.py:64
  416.9 18.6 %reduce-scatter.2.cloned.1.call-done = bf16[2048,1536]{1,0:T(8,128)(2,1)} async-done(((bf16[2048,3072]{1,0:T(8,128)(2,1)}), bf16[2048,1536]{1,0:T(8,128)(2,1)}) %reduce-scatter.2.cloned.1.call-update) | async-done | bytes 6291472 | tf_op jit(solution)/shard_map/reduce_scatter | solution.py:68
  435.5 6.0 all-to-all-start.4
  441.7 138.3 %all-to-all-done.4 = bf16[8,256,1536]{2,1,0:T(8,128)(2,1)} async-done(((bf16[8,256,1536]{2,1,0:T(8,128)(2,1)}), bf16[8,256,1536]{2,1,0:T(8,128)(2,1)}, u32[]{:S(2)}, u32[]{:S(2)}) %all-to-all-start.4) | async-done | bytes 6291488 | tf_op jit(solution)/shard_map/all_to_all | solution.py:72
  580.0 16.9 %gather_fusion.1 = bf16[2048,1536]{1,0:T(8,128)(2,1)} fusion(bf16[2048,1536]{1,0:T(8,128)(2,1)} %bitcast.18, s32[2048]{0:T(1024)S(1)} %broadcast_clamp_fusion), kind=kCustom, calls=%fused_computation.1 | custom fusion | bytes 12591104 | tf_op jit(solution)/shard_map/gather | solution.py:73
  596.9 14.2 %reshape.117 = f32[1024,2,1536]{2,1,0:T(2,128)} reshape(bf16[2048,1536]{1,0:T(8,128)(2,1)} %gather_fusion.1) | data formatting | bytes 18874368 | tf_op jit(solution)/shard_map/convert_element_type | solution.py:73
  611.1 22.4 %multiply_reduce_fusion = bf16[1024,1536]{1,0:T(8,128)(2,1)} fusion(f32[1024,2,1536]{2,1,0:T(2,128)} %reshape.117, f32[1024,2]{1,0:T(8,128)S(1)} %copy.27), kind=kLoop, calls=%fused_computation.7 | loop fusion | flops 4718592 | bytes 15736832 | tf_op jit(solution)/shard_map/reduce_sum | solution.py:74
  (45 shorter events, 10.2 us)
Async XLA Ops:
  20.9 4.6 copy-start
  63.1 7.5 %copy-start.4 = (f32[192]{0:T(256)S(1)}, f32[192]{0:T(256)}, u32[]{:S(2)}) copy-start(f32[192]{0:T(256)} %param.9) | copy-start | bytes 2308
  63.1 145.7 %all-to-all-start = ((bf16[8,128,3072]{2,1,0:T(8,128)(2,1)}), bf16[8,128,3072]{2,1,0:T(8,128)(2,1)}, u32[]{:S(2)}, u32[]{:S(2)}) async-start(bf16[8,128,3072]{2,1,0:T(8,128)(2,1)} %constant_dynamic-slice_fusion), calls=%async_computation | async-start | bytes 12582912 | tf_op jit(solution)/shard_map/all_to_all | solution.py:57
  70.5 5.4 copy-start.1
  70.5 138.3 %all-gather.10.cloned.1.call-start = ((), (), s32[]{:S(2)}) async-start(), calls=%async_computation.8 | async-start | bytes 3538944 | tf_op jit(solution)/shard_map/all_gather | solution.py:24
  75.1 137.4 %all-gather.12.cloned.1.call-start = ((), (), s32[]{:S(2)}) async-start(), calls=%async_computation.9 | async-start | bytes 3538944 | tf_op jit(solution)/shard_map/all_gather | solution.py:25
  75.9 195.0 %all-gather.14.cloned.1.call-start = ((), (), s32[]{:S(2)}) async-start(), calls=%async_computation.10 | async-start | bytes 3538944 | tf_op jit(solution)/shard_map/all_gather | solution.py:26
  77.1 308.3 %all-gather.8.cloned.1.call-start = ((), (), s32[]{:S(2)}) async-start(), calls=%async_computation.6 | async-start | bytes 18874368 | tf_op jit(solution)/shard_map/all_gather | solution.py:60
  208.8 57.7 %all-to-all-start.1 = ((bf16[8,2,192,384]{3,2,1,0:T(8,128)(2,1)}), bf16[8,2,192,384]{3,2,1,0:T(8,128)(2,1)S(1)}, u32[]{:S(2)}, u32[]{:S(2)}) async-start(bf16[8,2,192,384]{3,2,1,0:T(8,128)(2,1)} %bitcast.58), calls=%async_computation.1 | async-start | bytes 4718592 | tf_op jit(solution)/shard_map/all_to_all | solution.py:29
  266.5 57.8 %all-to-all-start.2 = ((bf16[8,2,192,384]{3,2,1,0:T(8,128)(2,1)}), bf16[8,2,192,384]{3,2,1,0:T(8,128)(2,1)}, u32[]{:S(2)}, u32[]{:S(2)}) async-start(bf16[8,2,192,384]{3,2,1,0:T(8,128)(2,1)} %bitcast.57), calls=%async_computation.2 | async-start | bytes 4718592 | tf_op jit(solution)/shard_map/all_to_all | solution.py:30
  324.3 57.8 %all-to-all-start.3 = ((bf16[8,2,192,384]{3,2,1,0:T(8,128)(2,1)}), bf16[8,2,192,384]{3,2,1,0:T(8,128)(2,1)}, u32[]{:S(2)}, u32[]{:S(2)}) async-start(bf16[8,2,192,384]{3,2,1,0:T(8,128)(2,1)} %bitcast.52), calls=%async_computation.3 | async-start | bytes 4718592 | tf_op jit(solution)/shard_map/all_to_all | solution.py:31
  328.7 106.8 %reduce-scatter.2.cloned.1.call-start = ((), (), s32[]{:S(2)}) async-start(), calls=%async_computation.7 | async-start | bytes 18874368 | tf_op jit(solution)/shard_map/reduce_scatter | solution.py:68
  333.9 51.5 %copy-start.2 = (bf16[8,2,192,384]{3,2,0,1:T(8,128)(2,1)S(1)}, bf16[8,2,192,384]{3,2,0,1:T(8,128)(2,1)}, u32[]{:S(2)}) copy-start(bf16[8,2,192,384]{3,2,0,1:T(8,128)(2,1)} %copy.31) | copy-start | bytes 7077892
  435.4 6.0 copy-start.3
  435.5 144.6 %all-to-all-start.4 = ((bf16[8,256,1536]{2,1,0:T(8,128)(2,1)}), bf16[8,256,1536]{2,1,0:T(8,128)(2,1)}, u32[]{:S(2)}, u32[]{:S(2)}) async-start(bf16[8,256,1536]{2,1,0:T(8,128)(2,1)} %bitcast.51), calls=%async_computation.5 | async-start | bytes 12582912 | tf_op jit(solution)/shard_map/all_to_all | solution.py:72
Sparse Core Ops, SparseCore 0:
  75.2 37.3 all-gather.9
  114.8 36.0 all-gather.11
  153.0 36.0 all-gather.13
  208.9 23.5 all-gather.7
  417.0 18.4 reduce-scatter.1
where the time goes:
time: 641 us; the launch traced here: 640 us
  waiting for transfers between devices  445 us (69%)
  local copies, waits for them, and re-layouts  82.1 us (13%)
  other arithmetic  41.4 us (6%)
  matrix products  31.4 us (5%)
  starting transfers between devices  26.3 us (4%)
  between operations  14 us (2%)
    all_to_all x1, waiting for transfers between devices, local(): lax.all_to_all(summed, 'fs', split_axis=0, concat_axis=0, tiled=True)  138 us
    all_to_all x1, waiting for transfers between devices, local(): lax.all_to_all(my_share, 'fs', split_axis=0, concat_axis=1, tiled=True)  132 us
    all_to_all x1, waiting for transfers between devices, local(): lax.all_to_all(gathered[0], 'fs', split_axis=0, concat_axis=2, tiled=True)  54 us
    all_to_all x1, waiting for transfers between devices, local(): lax.all_to_all(gathered[1], 'fs', split_axis=0, concat_axis=2, tiled=True)  53.4 us
    all_to_all x1, waiting for transfers between devices, local(): lax.all_to_all(gathered[2], 'fs', split_axis=0, concat_axis=2, tiled=True)  48.2 us
    gather x1, local copies, waits for them, and re-layouts, local(): outgoing = normed[source].reshape(experts, capacity, model_width)  26.6 us
    reduce_sum x1, other arithmetic, local(): jnp.sum(route_weight[:, :, None] * picked, axis=1).astype(jnp.bfloat16)  22.4 us
    dot_general x1, matrix products, local(): lax.dot_general(hidden, down_new[0], (((1,), (1,)), ((), ())), preferred_...  20.7 us
  transfers between devices with their start and end apart: 10, of which 6 were waited for; matrix products, arithmetic and copies ran while one was open for 2% of the time, Pallas kernels for 0%

commit v1 on v0

--- a/solution.py
+++ b/solution.py
@@ -9,7 +9,7 @@
 EPS = 1e-06
 
 
-def local(
+def local_spread(
     tokens, norm_gain, gate_weight, up_weight, down_weight, group_pick, expert_pick, route_weight
 ):
     scaled = norm_gain[None, :, None]
@@ -75,6 +75,100 @@
     return (combined, gate_new, up_new, down_new)
 
 
+def local_whole_group(
+    tokens, norm_gain, gate_weight, up_weight, down_weight, group_pick, expert_pick, route_weight
+):
+    experts, rows_dev, cols_dev = gate_weight.shape
+    tok_rows, model_width = tokens.shape
+    per_group = experts // GROUPS
+    n_tp = lax.axis_size("tp")
+    share = tok_rows // GROUPS // n_tp
+    own = share * GROUPS
+    columns = [[g * per_group + j for g in range(GROUPS)] for j in range(per_group)]
+    members = [[g * per_group + j for j in range(per_group)] for g in range(GROUPS)]
+
+    scaled = norm_gain[None, :, None]
+    served = []
+    for value in (scaled * gate_weight, scaled * up_weight, down_weight):
+        moved = lax.all_to_all(
+            value.astype(jnp.bfloat16), "fs", split_axis=0, concat_axis=1, tiled=True
+        )
+        served.append(lax.all_gather(moved, "gr", axis=1, tiled=True))
+    gate_new, up_new, down_new = served
+
+    onehot = (group_pick[None, :] == jnp.arange(GROUPS, dtype=jnp.int32)[:, None]).astype(
+        jnp.bfloat16
+    )
+    row = lax.broadcasted_iota(jnp.int32, (tok_rows, tok_rows), 0)
+    col = lax.broadcasted_iota(jnp.int32, (tok_rows, tok_rows), 1)
+    before = jnp.dot(onehot, (row < col).astype(jnp.bfloat16), preferred_element_type=jnp.float32)
+    rank = jnp.sum(onehot.astype(jnp.float32) * before, axis=0).astype(jnp.int32)
+    place = rank // share * own + group_pick * share + rank % share
+
+    as_float = tokens.astype(jnp.float32)
+    normed = (
+        as_float * lax.rsqrt(jnp.mean(as_float * as_float, axis=-1, keepdims=True) + EPS)
+    ).astype(jnp.bfloat16)
+    first = lax.axis_index("tp") * own
+    slots = first + lax.broadcasted_iota(jnp.int32, (own, tok_rows), 0)
+    select = (slots == place[None, :]).astype(jnp.bfloat16)
+    outgoing = jnp.dot(select, normed, preferred_element_type=jnp.float32).astype(jnp.bfloat16)
+
+    member = jnp.arange(per_group, dtype=jnp.int32)
+    by_member = jnp.sum(
+        jnp.where(expert_pick[:, :, None] == member, route_weight[:, :, None], 0.0), axis=1
+    )
+    weights_out = jnp.sum(
+        jnp.where((row == place[None, :])[None], by_member.T[:, None, :], 0.0), axis=2
+    )
+    weights_out = weights_out.reshape(per_group, n_tp, GROUPS, share)
+    weights_in = lax.all_to_all(
+        weights_out, "fs", split_axis=2, concat_axis=2, axis_index_groups=columns, tiled=True
+    )
+
+    landed = lax.all_to_all(
+        outgoing.reshape(GROUPS, share, model_width),
+        "fs",
+        split_axis=0,
+        concat_axis=0,
+        axis_index_groups=columns,
+        tiled=True,
+    )
+    shared = lax.all_gather(landed, "fs", axis=0, axis_index_groups=members)
+    arrived = lax.all_gather(shared, "tp", axis=0).reshape(-1, model_width)
+    gate_acts = jnp.dot(arrived, gate_new[0], preferred_element_type=jnp.float32)
+    up_acts = jnp.dot(arrived, up_new[0], preferred_element_type=jnp.float32)
+    hidden = (jax.nn.silu(gate_acts) * up_acts).astype(jnp.bfloat16)
+    partial_value = lax.dot_general(
+        hidden, down_new[0], (((1,), (1,)), ((), ())), preferred_element_type=jnp.float32
+    ).astype(jnp.bfloat16)
+    summed = lax.psum_scatter(partial_value, "tp", scatter_dimension=1, tiled=True)
+    width = summed.shape[1]
+    paired = lax.all_to_all(
+        summed.reshape(n_tp, per_group, GROUPS, share, width),
+        "fs",
+        split_axis=1,
+        concat_axis=1,
+        axis_index_groups=members,
+        tiled=True,
+    )
+    mixed = sum(
+        weights_in[j][..., None] * paired[:, j].astype(jnp.float32) for j in range(per_group)
+    ).astype(jnp.bfloat16)
+    returned = lax.all_to_all(
+        mixed, "fs", split_axis=1, concat_axis=1, axis_index_groups=columns, tiled=True
+    ).reshape(tok_rows, width)
+    restore = (col == place[:, None]).astype(jnp.bfloat16)
+    combined = jnp.dot(restore, returned, preferred_element_type=jnp.float32).astype(jnp.bfloat16)
+    return (combined, gate_new, up_new, down_new)
+
+
+def local(tokens, norm_gain, gate, up, down, group_pick, expert_pick, route_weight):
+    whole_group = gate.shape[0] // GROUPS == expert_pick.shape[1]
+    body = local_whole_group if whole_group else local_spread
+    return body(tokens, norm_gain, gate, up, down, group_pick, expert_pick, route_weight)
+
+
 def solution(mesh):
     in_specs = (
         P(("gr", "fs"), None),

time: 641 us -> 547 us (0.85)
  blocking collectives: 0 us -> 250 us
  waiting for transfers between devices: 445 us -> 199 us
  local copies, waits for them, and re-layouts: 82.1 us -> 15.7 us
  other arithmetic: 41.4 us -> 12.7 us
  starting transfers between devices: 26.3 us -> 11.3 us
  matrix products: 31.4 us -> 43.3 us
    all_to_all x5 -> x2, waiting for transfers between devices: 425 us -> 70.6 us  [the longest x1 70.6 us: local_whole_group(): lax.all_to_all(summed.reshape(n_tp, per_group, GROUPS, share, width), 'fs...]
    all_to_all x0 -> x5, blocking collectives: none -> 250 us  [the longest x3 98 us: local_whole_group(): lax.all_to_all(value.astype(jnp.bfloat16), 'fs', split_axis=0, concat_axi...]
    all_gather x4 -> x5, waiting for transfers between devices: 0.05 us -> 117 us  [the longest x3 63.5 us: local_whole_group(): served.append(lax.all_gather(moved, 'gr', axis=1, tiled=True))]
    gather x2 -> x0, local copies, waits for them, and re-layouts: 43.5 us -> none  [the longest x1 26.6 us: local(): outgoing = normed[source].reshape(experts, capacity, model_width)]
    reduce_sum x3, other arithmetic: 26.7 us -> 5.41 us  [the longest x1 4.08 us: local_whole_group(): jnp.mean(as_float * as_float, axis=-1, keepdims=True) + EPS]
    all_to_all x5 -> x2, starting transfers between devices: 25.9 us -> 10.9 us  [the longest x1 6.28 us: local_whole_group(): lax.all_to_all(summed.reshape(n_tp, per_group, GROUPS, share, width), 'fs...]
    convert_element_type x1, local copies, waits for them, and re-layouts: 14.2 us -> 0.2 us  [local_whole_group(): mixed = sum((weights_in[j][..., None] * paired[:, j].astype(jnp.float32)...]
    dot_general x2 -> x5, matrix products: 31.4 us -> 43.3 us  [the longest x1 20.2 us: local_whole_group(): lax.dot_general(hidden, down_new[0], (((1,), (1,)), ((), ())), preferred_...]
  transfers between devices with their start and end apart: 10 -> 8, of which waited for: 6 -> 5; matrix products, arithmetic and copies ran while one was open for 2% -> 4% of each run, Pallas kernels for 0% -> 0%
where the time goes in v1:
time: 547 us; the launch traced here: 546 us
  blocking collectives  250 us (46%)
  waiting for transfers between devices  199 us (36%)
  matrix products  43.3 us (8%)
  local copies, waits for them, and re-layouts  15.7 us (3%)
  between operations  14.3 us (3%)
  other arithmetic  12.7 us (2%)
  starting transfers between devices  11.3 us (2%)
    all_to_all x3, blocking collectives, local_whole_group(): lax.all_to_all(value.astype(jnp.bfloat16), 'fs', split_axis=0, concat_axi...  98 us
    all_to_all x1, blocking collectives, local_whole_group(): lax.all_to_all(outgoing.reshape(GROUPS, share, model_width), 'fs', split_...  76.9 us
    all_to_all x1, blocking collectives, local_whole_group(): lax.all_to_all(mixed, 'fs', split_axis=1, concat_axis=1, axis_index_group...  74.7 us
    all_to_all x1, waiting for transfers between devices, local_whole_group(): lax.all_to_all(summed.reshape(n_tp, per_group, GROUPS, share, width), 'fs...  70.6 us
    all_gather x3, waiting for transfers between devices, local_whole_group(): served.append(lax.all_gather(moved, 'gr', axis=1, tiled=True))  63.5 us
    all_gather x1, waiting for transfers between devices, local_whole_group(): shared = lax.all_gather(landed, 'fs', axis=0, axis_index_groups=members)  53.4 us
    dot_general x1, matrix products, local_whole_group(): lax.dot_general(hidden, down_new[0], (((1,), (1,)), ((), ())), preferred_...  20.2 us
    reduce_scatter x1, waiting for transfers between devices, local_whole_group(): lax.psum_scatter(partial_value, 'tp', scatter_dimension=1, tiled=True)  11.5 us
  transfers between devices with their start and end apart: 8, of which 5 were waited for; matrix products, arithmetic and copies ran while one was open for 4% of the time, Pallas kernels for 0%

profile of v1, /device:TPU:0, one launch (start us, length us, event | category | flops | bytes accessed | tf_op | source)
XLA Modules:
  0.0 546.2 jit_solution(11293096170578549441)
XLA Ops:
  9.0 4.1 fusion
  13.1 6.8 %fusion.7 = bf16[512,3072]{1,0:T(8,128)(2,1)S(1)} fusion(bf16[1024,3072]{1,0:T(8,128)(2,1)} %param.8, f32[1024]{0:T(1024)S(1)} %add_rsqrt_fusion, s32[1024]{0:T(1024)S(1)} %fusion.30, s32[512]{0:T(512)S(1)} %iota_add_fusion), kind=kOutput, calls=%fused_computation.12 | convolution fusion | flops 3232759808 | bytes 9447424 | tf_op jit(solution)/shard_map/dot_general | solution.py:115
  19.9 76.9 %all_to_all.56 = bf16[4,128,3072]{2,1,0:T(8,128)(2,1)} all-to-all(bf16[4,128,3072]{2,1,0:T(8,128)(2,1)S(1)} %bitcast.41), channel_id=1, replica_groups={{0,4,8,12},{2,6,10,14},{1,5,9,13},{3,7,11,15},{16,20,24,28},{18,22,26,3..., dimensions={0} | all-to-all | bytes 6291456 | tf_op jit(solution)/shard_map/all_to_all | solution.py:129
  96.9 1.6 copy-done.4
  98.5 2.2 multiply_convert_fusion.1
  100.7 32.4 %all_to_all.57 = bf16[8,192,384]{2,1,0:T(8,128)(2,1)} all-to-all(bf16[8,192,384]{2,1,0:T(8,128)(2,1)S(1)} %get-tuple-element.7), channel_id=1, replica_groups=mesh['gr'=2,'fs'=8,'tp'=2] {'fs'}, dimensions={0} | all-to-all | bytes 2359296 | tf_op jit(solution)/shard_map/all_to_all | solution.py:93
  133.2 53.4 %all-gather.14.cloned.1.call-done = bf16[8,128,3072]{2,1,0:T(8,128)(2,1)} async-done(((bf16[4,128,3072]{2,1,0:T(8,128)(2,1)}), bf16[8,128,3072]{2,1,0:T(8,128)(2,1)}) %all-gather.14.cloned.1.call-update) | async-done | bytes 6291472 | tf_op jit(solution)/shard_map/all_gather | solution.py:137
  186.8 33.6 %all_to_all.58 = bf16[8,192,384]{2,1,0:T(8,128)(2,1)} all-to-all(bf16[8,192,384]{2,1,0:T(8,128)(2,1)S(1)} %get-tuple-element.6), channel_id=1, replica_groups=mesh['gr'=2,'fs'=8,'tp'=2] {'fs'}, dimensions={0} | all-to-all | bytes 2359296 | tf_op jit(solution)/shard_map/all_to_all | solution.py:93
  220.6 31.9 %all_to_all.59 = bf16[8,192,384]{2,1,0:T(8,128)(2,1)} all-to-all(bf16[8,192,384]{2,1,0:T(8,128)(2,1)S(1)} %convert_element_type.63), channel_id=1, replica_groups=mesh['gr'=2,'fs'=8,'tp'=2] {'fs'}, dimensions={0} | all-to-all | bytes 2359296 | tf_op jit(solution)/shard_map/all_to_all | solution.py:93
  252.9 10.3 %fusion.16 = f32[2048,384]{1,0:T(8,128)S(1)} fusion(bf16[2048,3072]{1,0:T(8,128)(2,1)} %bitcast.44, bf16[1,3072,384]{2,1,0:T(8,128)(2,1)} %all-gather.8.cloned.1.call-done), kind=kOutput, calls=%fused_computation.24 | convolution fusion | flops 4831838208 | bytes 18087936 | tf_op jit(solution)/shard_map/dot_general | solution.py:139
  263.2 26.0 %all-gather.10.cloned.1.call-done = bf16[1,3072,384]{2,1,0:T(8,128)(2,1)} async-done(((bf16[1,1536,384]{2,1,0:T(8,128)(2,1)}), bf16[1,3072,384]{2,1,0:T(8,128)(2,1)}) %all-gather.10.cloned.1.call-update) | async-done | bytes 2359312 | tf_op jit(solution)/shard_map/all_gather | solution.py:96
  289.2 37.5 %all-gather.12.cloned.1.call-done = bf16[1,3072,384]{2,1,0:T(8,128)(2,1)} async-done(((bf16[1,1536,384]{2,1,0:T(8,128)(2,1)}), bf16[1,3072,384]{2,1,0:T(8,128)(2,1)}) %all-gather.12.cloned.1.call-update) | async-done | bytes 2359312 | tf_op jit(solution)/shard_map/all_gather | solution.py:96
  326.6 20.2 %convolution_convert_fusion = bf16[2048,3072]{1,0:T(8,128)(2,1)} fusion(bf16[1,3072,384]{2,1,0:T(8,128)(2,1)} %all-gather.12.cloned.1.call-done, f32[2048,384]{1,0:T(8,128)S(1)} %fusion.16, bf16[2048,3072]{1,0:T(8,128)(2,1)} %bitcast.45, bf16[1,3072,384]{2,1,0:T(8,128)(2,1)} %all-gather.10.cloned.1.call-done), kind=kOutput, calls=%fused_computation.4 | convolution fusion | flops 9674686464 | bytes 33030144 | tf_op jit(solution)/shard_map/dot_general | solution.py:142
  350.3 4.6 all-to-all-start
  354.9 11.5 %reduce-scatter.2.cloned.1.call-done = bf16[2048,1536]{1,0:T(8,128)(2,1)} async-done(((bf16[2048,3072]{1,0:T(8,128)(2,1)}), bf16[2048,1536]{1,0:T(8,128)(2,1)}) %reduce-scatter.2.cloned.1.call-update) | async-done | bytes 6291472 | tf_op jit(solution)/shard_map/reduce_scatter | solution.py:145
  366.4 6.0 %copy.31 = bf16[2,2,4,128,1536]{4,3,2,0,1:T(8,128)(2,1)} copy(bf16[2,2,4,128,1536]{4,3,2,1,0:T(8,128)(2,1)} %bitcast.37) | data formatting | bytes 12582912 | tf_op jit(solution)/shard_map/reshape | solution.py:148
  372.4 6.3 %all-to-all-start.5 = ((bf16[2,2,4,128,1536]{4,3,2,0,1:T(8,128)(2,1)}), bf16[2,2,4,128,1536]{4,3,2,0,1:T(8,128)(2,1)}, u32[]{:S(2)}, u32[]{:S(2)}) async-start(bf16[2,2,4,128,1536]{4,3,2,0,1:T(8,128)(2,1)} %copy.31), calls=%async_computation.6 | async-start | bytes 12582912 | tf_op jit(solution)/shard_map/all_to_all | solution.py:147
  378.7 70.6 %all-to-all-done.5 = bf16[2,2,4,128,1536]{4,3,2,0,1:T(8,128)(2,1)} async-done(((bf16[2,2,4,128,1536]{4,3,2,0,1:T(8,128)(2,1)}), bf16[2,2,4,128,1536]{4,3,2,0,1:T(8,128)(2,1)}, u32[]{:S(2)}, u32[]{:S(2)}) %all-to-all-start.5) | async-done | bytes 6291488 | tf_op jit(solution)/shard_map/all_to_all | solution.py:147
  449.3 3.5 fusion.5
  453.0 74.7 %all_to_all.60 = bf16[2,4,128,1536]{3,2,0,1:T(8,128)(2,1)S(1)} all-to-all(bf16[2,4,128,1536]{3,2,0,1:T(8,128)(2,1)S(1)} %copy.33), channel_id=1, replica_groups={{0,4,8,12},{2,6,10,14},{1,5,9,13},{3,7,11,15},{16,20,24,28},{18,22,26,3..., dimensions={1} | all-to-all | bytes 6291456 | tf_op jit(solution)/shard_map/all_to_all | solution.py:158
  527.9 5.0 fusion.12
  532.9 1.4 copy.38
  535.4 1.4 copy.39
  537.9 1.4 copy.40
  (45 shorter events, 8.6 us)
Async XLA Ops:
  7.2 179.5 %all-gather.14.cloned.1.call-start = ((), (), s32[]{:S(2)}) async-start(), calls=%async_computation.12 | async-start | bytes 9437184 | tf_op jit(solution)/shard_map/all_gather | solution.py:137
  96.9 1.7 copy-start.4
  96.9 1.7 copy-start.7
  96.9 156.0 %all-gather.8.cloned.1.call-start = ((), (), s32[]{:S(2)}) async-start(), calls=%async_computation.8 | async-start | bytes 3538944 | tf_op jit(solution)/shard_map/all_gather | solution.py:96
  133.2 119.7 %all-gather.16.cloned.1.call-start = ((), (), s32[]{:S(2)}) async-start(), calls=%async_computation.13 | async-start | bytes 18874368 | tf_op jit(solution)/shard_map/all_gather | solution.py:138
  186.7 33.8 %copy-start = (f32[8,192,384]{2,1,0:T(8,128)S(1)}, f32[8,192,384]{2,1,0:T(8,128)}, u32[]{:S(2)}) copy-start(f32[8,192,384]{2,1,0:T(8,128)} %param.12) | copy-start | bytes 7077892
  186.7 102.5 %all-gather.10.cloned.1.call-start = ((), (), s32[]{:S(2)}) async-start(), calls=%async_computation.9 | async-start | bytes 3538944 | tf_op jit(solution)/shard_map/all_gather | solution.py:96
  220.4 106.2 %all-gather.12.cloned.1.call-start = ((), (), s32[]{:S(2)}) async-start(), calls=%async_computation.10 | async-start | bytes 3538944 | tf_op jit(solution)/shard_map/all_gather | solution.py:96
  252.6 113.8 %reduce-scatter.2.cloned.1.call-start = ((), (), s32[]{:S(2)}) async-start(), calls=%async_computation.11 | async-start | bytes 18874368 | tf_op jit(solution)/shard_map/reduce_scatter | solution.py:145
  346.8 0.7 copy-start.5
  346.8 0.7 copy-start.6
  350.3 22.1 %all-to-all-start = ((f32[2,2,4,128]{3,1,0,2:T(2,128)}), f32[2,2,4,128]{3,1,0,2:T(2,128)S(1)}, u32[]{:S(2)}, u32[]{:S(2)}) async-start(f32[2,2,4,128]{3,1,0,2:T(2,128)} %copy.29), calls=%async_computation | async-start | bytes 16384 | tf_op jit(solution)/shard_map/all_to_all | solution.py:125
  372.4 76.9 %all-to-all-start.5 = ((bf16[2,2,4,128,1536]{4,3,2,0,1:T(8,128)(2,1)}), bf16[2,2,4,128,1536]{4,3,2,0,1:T(8,128)(2,1)}, u32[]{:S(2)}, u32[]{:S(2)}) async-start(bf16[2,2,4,128,1536]{4,3,2,0,1:T(8,128)(2,1)} %copy.31), calls=%async_computation.6 | async-start | bytes 12582912 | tf_op jit(solution)/shard_map/all_to_all | solution.py:147
  527.9 5.0 copy-start.1
  532.9 2.5 copy-start.2
  535.4 2.5 copy-start.3
Sparse Core Ops, SparseCore 0:
  97.0 89.6 all-gather.13
  188.2 35.9 all-gather.7
  225.8 24.6 all-gather.15
  251.9 37.2 all-gather.9
  290.6 36.0 all-gather.11
  347.0 19.3 reduce-scatter.1

commit v2 on v1

--- a/solution.py
+++ b/solution.py
@@ -1,6 +1,8 @@
 import jax
 import jax.numpy as jnp
 from jax import lax
+from jax.experimental import pallas as pl
+from jax.experimental.pallas import tpu as pltpu
 from jax.sharding import PartitionSpec as P
 
 GROUPS = 4
@@ -75,6 +77,218 @@
     return (combined, gate_new, up_new, down_new)
 
 
+def greet(peers):
+    barrier = pltpu.get_barrier_semaphore()
+    for peer in peers:
+        pl.semaphore_signal(barrier, inc=1, device_id=peer, device_id_type=pl.DeviceIdType.MESH)
+    pl.semaphore_wait(barrier, len(peers))
+
+
+def remote(src, dst, send, recv, peer):
+    return pltpu.make_async_remote_copy(
+        src_ref=src,
+        dst_ref=dst,
+        send_sem=send,
+        recv_sem=recv,
+        device_id=peer,
+        device_id_type=pl.DeviceIdType.MESH,
+    )
+
+
+def dispatch(tokens_out, gate_out, up_out, down_out):
+    groups, share, width = tokens_out.shape
+    n_fs, rows, cols = gate_out.shape
+    n_gr, n_tp = lax.axis_size("gr"), lax.axis_size("tp")
+    members = n_fs // groups
+    n_weights = 3
+
+    def kernel(tok, w0, w1, w2, arrived, s0, s1, s2, sends, local, rz, ry, rt, rw, rg):
+        fs, gr, tp = lax.axis_index("fs"), lax.axis_index("gr"), lax.axis_index("tp")
+        g, j = fs // members, fs % members
+        out_w, in_w = (w0, w1, w2), (s0, s1, s2)
+        fs_peers = [{"fs": (fs + s) % n_fs} for s in range(1, n_fs)]
+        gr_peers = [{"gr": (gr + s) % n_gr} for s in range(1, n_gr)]
+        tp_peers = [{"tp": (tp + s) % n_tp} for s in range(1, n_tp)]
+        greet(fs_peers + gr_peers + tp_peers)
+        started = []
+
+        def send(src, dst, recv, peer):
+            copy = remote(src, dst, sends.at[len(started)], recv, peer)
+            copy.start()
+            started.append(copy)
+
+        def landed(ref, recv):
+            remote(ref, ref, sends.at[0], recv, tp_peers[0]).wait_recv()
+
+        for s in range(1, groups):
+            z = (g + s) % groups
+            send(tok.at[z], arrived.at[tp, j, g], rz.at[g], {"fs": z * members + j})
+        for s in range(1, n_fs):
+            d = (fs + s) % n_fs
+            for w in range(n_weights):
+                send(out_w[w].at[d], in_w[w].at[gr, fs], rw.at[w, fs], {"fs": d})
+        locals_ = [pltpu.make_async_copy(tok.at[g], arrived.at[tp, j, g], local.at[n_weights])]
+        for w in range(n_weights):
+            locals_.append(
+                pltpu.make_async_copy(out_w[w].at[fs], in_w[w].at[gr, fs], local.at[w])
+            )
+        for copy in locals_:
+            copy.start()
+
+        for s in range(groups):
+            z = (g + groups - s) % groups
+            slot = arrived.at[tp, j, z]
+            if s:
+                landed(slot, rz.at[z])
+            source = slot if s else tok.at[g]
+            for m in range(1, members):
+                send(source, slot, ry.at[j, z], {"fs": g * members + (j + m) % members})
+            for peer in tp_peers:
+                send(source, slot, rt.at[j, z], peer)
+        for s in range(n_fs):
+            d = (fs + n_fs - s) % n_fs
+            for w in range(n_weights):
+                slot = in_w[w].at[gr, d]
+                if s:
+                    landed(slot, rw.at[w, d])
+                for peer in gr_peers:
+                    send(slot if s else out_w[w].at[fs], slot, rg.at[w, d], peer)
+        for m in range(1, members):
+            other = (j + m) % members
+            for s in range(groups):
+                z = (g + groups - s) % groups
+                slot = arrived.at[tp, other, z]
+                landed(slot, ry.at[other, z])
+                for peer in tp_peers:
+                    send(slot, slot, rt.at[other, z], peer)
+        for t in range(1, n_tp):
+            for m in range(members):
+                for z in range(groups):
+                    landed(arrived.at[(tp + t) % n_tp, m, z], rt.at[m, z])
+        for q in range(1, n_gr):
+            for w in range(n_weights):
+                for d in range(n_fs):
+                    landed(in_w[w].at[(gr + q) % n_gr, d], rg.at[w, d])
+        for copy in locals_:
+            copy.wait()
+        for copy in started:
+            copy.wait_send()
+
+    n_sends = (
+        groups - 1
+        + n_weights * (n_fs - 1)
+        + groups * (members - 1 + n_tp - 1)
+        + n_weights * n_fs * (n_gr - 1)
+        + groups * (members - 1) * (n_tp - 1)
+    )
+    served = jax.ShapeDtypeStruct((n_gr, n_fs, rows, cols), jnp.bfloat16)
+    dma = pltpu.SemaphoreType.DMA
+    out = pl.pallas_call(
+        kernel,
+        out_shape=(
+            jax.ShapeDtypeStruct((n_tp, members, groups, share, width), jnp.bfloat16),
+            served,
+            served,
+            served,
+        ),
+        in_specs=[pl.BlockSpec(memory_space=pltpu.VMEM)] * 4,
+        out_specs=[pl.BlockSpec(memory_space=pl.ANY)] * 4,
+        scratch_shapes=[
+            dma((n_sends,)),
+            dma((n_weights + 1,)),
+            dma((groups,)),
+            dma((members, groups)),
+            dma((members, groups)),
+            dma((n_weights, n_fs)),
+            dma((n_weights, n_fs)),
+        ],
+        compiler_params=pltpu.CompilerParams(
+            collective_id=0, has_side_effects=True, vmem_limit_bytes=60 * 2**20
+        ),
+        name="dispatch",
+    )(tokens_out, gate_out, up_out, down_out)
+    return out[0], [x.reshape(1, -1, cols) for x in out[1:]]
+
+
+def give_back(summed, weights_in):
+    n_tp, members, groups, share, width = summed.shape
+
+    def kernel(own, weight, home, others, mixed, send_y, recv_y, send_z, recv_z):
+        fs = lax.axis_index("fs")
+        g, j = fs // members, fs % members
+        mates = [{"fs": g * members + (j + m) % members} for m in range(1, members)]
+        greet(mates + [{"fs": (g + s) % groups * members + j} for s in range(1, groups)])
+        order = [s % groups for s in range(1, groups + 1)]
+        copies = []
+        for s in order:
+            z = (g + s) % groups
+            for t in range(n_tp):
+                for m in range(1, members):
+                    copy = remote(
+                        own.at[t, (j + m) % members, z],
+                        others.at[members - m - 1, t, z],
+                        send_y.at[m - 1, t, s],
+                        recv_y.at[members - m - 1, t, z],
+                        mates[m - 1],
+                    )
+                    copy.start()
+                    copies.append(copy)
+        for s in order:
+            z = (g + s) % groups
+            for t in range(n_tp):
+                total = weight[j, t, z] * own[t, j, z].astype(jnp.float32)
+                for m in range(1, members):
+                    slot = others.at[m - 1, t, z]
+                    remote(
+                        slot, slot, send_y.at[0, 0, 0], recv_y.at[m - 1, t, z], mates[m - 1]
+                    ).wait_recv()
+                    total += weight[(j + m) % members, t, z] * others[m - 1, t, z].astype(
+                        jnp.float32
+                    )
+                if s:
+                    mixed[s - 1, t] = total.astype(jnp.bfloat16)
+                    copy = remote(
+                        mixed.at[s - 1, t],
+                        home.at[t, g],
+                        send_z.at[t, s - 1],
+                        recv_z.at[t, g],
+                        {"fs": z * members + j},
+                    )
+                    copy.start()
+                    copies.append(copy)
+                else:
+                    home[t, g] = total.astype(jnp.bfloat16)
+        for s in range(1, groups):
+            z = (g + s) % groups
+            for t in range(n_tp):
+                slot = home.at[t, z]
+                remote(
+                    slot, slot, send_z.at[0, 0], recv_z.at[t, z], {"fs": z * members + j}
+                ).wait_recv()
+        for copy in copies:
+            copy.wait_send()
+
+    dma = pltpu.SemaphoreType.DMA
+    return pl.pallas_call(
+        kernel,
+        out_shape=jax.ShapeDtypeStruct((n_tp, groups, share, width), jnp.bfloat16),
+        in_specs=[pl.BlockSpec(memory_space=pltpu.VMEM)] * 2,
+        out_specs=pl.BlockSpec(memory_space=pltpu.VMEM),
+        scratch_shapes=[
+            pltpu.VMEM((members - 1, n_tp, groups, share, width), jnp.bfloat16),
+            pltpu.VMEM((groups - 1, n_tp, share, width), jnp.bfloat16),
+            dma((members - 1, n_tp, groups)),
+            dma((members - 1, n_tp, groups)),
+            dma((n_tp, groups - 1)),
+            dma((n_tp, groups)),
+        ],
+        compiler_params=pltpu.CompilerParams(
+            collective_id=1, has_side_effects=True, vmem_limit_bytes=60 * 2**20
+        ),
+        name="give_back",
+    )(summed, weights_in)
+
+
 def local_whole_group(
     tokens, norm_gain, gate_weight, up_weight, down_weight, group_pick, expert_pick, route_weight
 ):
@@ -85,16 +299,11 @@
     share = tok_rows // GROUPS // n_tp
     own = share * GROUPS
     columns = [[g * per_group + j for g in range(GROUPS)] for j in range(per_group)]
-    members = [[g * per_group + j for j in range(per_group)] for g in range(GROUPS)]
 
     scaled = norm_gain[None, :, None]
-    served = []
-    for value in (scaled * gate_weight, scaled * up_weight, down_weight):
-        moved = lax.all_to_all(
-            value.astype(jnp.bfloat16), "fs", split_axis=0, concat_axis=1, tiled=True
-        )
-        served.append(lax.all_gather(moved, "gr", axis=1, tiled=True))
-    gate_new, up_new, down_new = served
+    to_serve = [
+        value.astype(jnp.bfloat16) for value in (scaled * gate_weight, scaled * up_weight, down_weight)
+    ]
 
     onehot = (group_pick[None, :] == jnp.arange(GROUPS, dtype=jnp.int32)[:, None]).astype(
         jnp.bfloat16
@@ -126,16 +335,10 @@
         weights_out, "fs", split_axis=2, concat_axis=2, axis_index_groups=columns, tiled=True
     )
 
-    landed = lax.all_to_all(
-        outgoing.reshape(GROUPS, share, model_width),
-        "fs",
-        split_axis=0,
-        concat_axis=0,
-        axis_index_groups=columns,
-        tiled=True,
-    )
-    shared = lax.all_gather(landed, "fs", axis=0, axis_index_groups=members)
-    arrived = lax.all_gather(shared, "tp", axis=0).reshape(-1, model_width)
+    arrived, (gate_new, up_new, down_new) = dispatch(
+        outgoing.reshape(GROUPS, share, model_width), *to_serve
+    )
+    arrived = arrived.reshape(-1, model_width)
     gate_acts = jnp.dot(arrived, gate_new[0], preferred_element_type=jnp.float32)
     up_acts = jnp.dot(arrived, up_new[0], preferred_element_type=jnp.float32)
     hidden = (jax.nn.silu(gate_acts) * up_acts).astype(jnp.bfloat16)
@@ -144,19 +347,8 @@
     ).astype(jnp.bfloat16)
     summed = lax.psum_scatter(partial_value, "tp", scatter_dimension=1, tiled=True)
     width = summed.shape[1]
-    paired = lax.all_to_all(
-        summed.reshape(n_tp, per_group, GROUPS, share, width),
-        "fs",
-        split_axis=1,
-        concat_axis=1,
-        axis_index_groups=members,
-        tiled=True,
-    )
-    mixed = sum(
-        weights_in[j][..., None] * paired[:, j].astype(jnp.float32) for j in range(per_group)
-    ).astype(jnp.bfloat16)
-    returned = lax.all_to_all(
-        mixed, "fs", split_axis=1, concat_axis=1, axis_index_groups=columns, tiled=True
+    returned = give_back(
+        summed.reshape(n_tp, per_group, GROUPS, share, width), weights_in[..., None]
     ).reshape(tok_rows, width)
     restore = (col == place[:, None]).astype(jnp.bfloat16)
     combined = jnp.dot(restore, returned, preferred_element_type=jnp.float32).astype(jnp.bfloat16)

time: 547 us -> 374 us (0.68)
  Pallas kernels: 0 us -> 257 us
  blocking collectives: 250 us -> 0 us
  waiting for transfers between devices: 199 us -> 9.25 us
  starting transfers between devices: 11.3 us -> 27.3 us
  local copies, waits for them, and re-layouts: 15.7 us -> 8.01 us
    pallas_call x0 -> x2, Pallas kernels: none -> 257 us  [the longest x1 170 us: dispatch(): pl.pallas_call(kernel, out_shape=(jax.ShapeDtypeStruct((n_tp, members, gr...]
    all_to_all x5 -> x0, blocking collectives: 250 us -> none  [the longest x3 98 us: local_whole_group(): lax.all_to_all(value.astype(jnp.bfloat16), 'fs', split_axis=0, concat_axi...]
    all_gather x5 -> x0, waiting for transfers between devices: 117 us -> none  [the longest x3 63.5 us: local_whole_group(): served.append(lax.all_gather(moved, 'gr', axis=1, tiled=True))]
    all_to_all x1 -> x0, waiting for transfers between devices: 70.6 us -> none  [local_whole_group(): lax.all_to_all(summed.reshape(n_tp, per_group, GROUPS, share, width), 'fs...]
    all_to_all x1, starting transfers between devices: 4.6 us -> 27.3 us  [local_whole_group(): lax.all_to_all(weights_out, 'fs', split_axis=2, concat_axis=2, axis_index...]
    reduce_scatter x1, waiting for transfers between devices: 11.5 us -> 3.64 us  [local_whole_group(): lax.psum_scatter(partial_value, 'tp', scatter_dimension=1, tiled=True)]
    all_to_all x1 -> x0, starting transfers between devices: 6.28 us -> none  [local_whole_group(): lax.all_to_all(summed.reshape(n_tp, per_group, GROUPS, share, width), 'fs...]
    reshape x1 -> x0, local copies, waits for them, and re-layouts: 5.97 us -> none  [local_whole_group(): summed.reshape(n_tp, per_group, GROUPS, share, width)]
  transfers between devices with their start and end apart: 8 -> 2, of which waited for: 5 -> 2; matrix products, arithmetic and copies ran while one was open for 4% -> 1% of each run, Pallas kernels for 0% -> 0%
where the time goes in v2:
time: 374 us
  Pallas kernels  257 us (69%)
  matrix products  47.7 us (13%)
  starting transfers between devices  27.3 us (7%)
  between operations  14.1 us (4%)
  other arithmetic  10.2 us (3%)
  waiting for transfers between devices  9.25 us (2%)
  local copies, waits for them, and re-layouts  8.01 us (2%)
    pallas_call x1, Pallas kernels, dispatch(): pl.pallas_call(kernel, out_shape=(jax.ShapeDtypeStruct((n_tp, members, gr...  170 us
    pallas_call x1, Pallas kernels, give_back(): pl.pallas_call(kernel, out_shape=jax.ShapeDtypeStruct((n_tp, groups, shar...  87.5 us
    all_to_all x1, starting transfers between devices, local_whole_group(): lax.all_to_all(weights_out, 'fs', split_axis=2, concat_axis=2, axis_index...  27.3 us
    dot_general x1, matrix products, local_whole_group(): lax.dot_general(hidden, down_new[0], (((1,), (1,)), ((), ())), preferred_...  19.9 us
    dot_general x1, matrix products, local_whole_group(): jnp.dot(arrived, gate_new[0], preferred_element_type=jnp.float32)  11.6 us
    dot_general x1, matrix products, local_whole_group(): jnp.dot(select, normed, preferred_element_type=jnp.float32)  8.08 us
  transfers between devices with their start and end apart: 2, of which 2 were waited for; matrix products, arithmetic and copies ran while one was open for 1% of the time, Pallas kernels for 0%

profile of v2, /device:TPU:0, one launch (start us, length us, event | category | flops | bytes accessed | tf_op | source)
XLA Modules:
  0.0 373.8 jit_solution(15486868101043230147)
XLA Ops:
  7.2 0.0 reduce-scatter.2.cloned.1.call-start
  7.2 1.1 fusion.15
  8.3 0.7 fusion.23
  9.0 4.2 %fusion = f32[1024]{0:T(1024)S(1)} fusion(bf16[1024,3072]{1,0:T(8,128)(2,1)} %param.8), kind=kLoop, calls=%fused_computation.2 | loop fusion | flops 9436160 | bytes 6295552 | tf_op jit(solution)/shard_map/reduce_sum | solution.py:319
  13.3 1.2 convert_element_type.47.w2
  14.4 8.1 %fusion.5 = bf16[512,3072]{1,0:T(8,128)(2,1)} fusion(bf16[1024,3072]{1,0:T(8,128)(2,1)} %param.8, f32[1024]{0:T(1024)S(1)} %add_rsqrt_fusion, s32[1024]{0:T(1024)S(1)} %fusion.23, s32[512]{0:T(512)S(1)} %iota_add_fusion), kind=kOutput, calls=%fused_computation.8 | convolution fusion | flops 3232759808 | bytes 9447424 | tf_op jit(solution)/shard_map/dot_general | solution.py:324
  22.5 2.0 multiply_convert_fusion.1
  24.5 169.6 %dispatch.1 = (bf16[2,2,4,128,3072]{4,3,2,1,0:T(8,128)(2,1)}, bf16[2,8,192,384]{3,2,1,0:T(8,128)(2,1)}, bf16[2,8,192,384]{3,2,1,0:T(8,128)(2,1)}, bf16[2,8,192,384]{3,2,1,0:T(8,128)(2,1)}) custom-call(bf16[4,128,3072]{2,1,0:T(8,128)(2,1)} %bitcast.19, bf16[8,192,384]{2,1,0:T(8,128)(2,1)} %get-tuple-element.13.w0, bf16[8,192,384]{2,1,0:T(8,128)(2,1)} %get-tuple-element.12.w1, ...), custom_call_target="tpu_custom_call" | custom-call | tf_op jit(solution)/shard_map/dispatch/pallas_call | solution.py:186
  194.1 11.6 %fusion.29 = f32[2048,384]{1,0:T(8,128)} fusion(bf16[2048,3072]{1,0:T(8,128)(2,1)} %bitcast.29, bf16[3072,384]{1,0:T(8,128)(2,1)} %bitcast.25), kind=kOutput, calls=%fused_computation.47 | convolution fusion | flops 4831838208 | bytes 18087936 | tf_op jit(solution)/shard_map/dot_general | solution.py:342
  205.7 19.9 %convolution_convert_fusion = bf16[2048,3072]{1,0:T(8,128)(2,1)} fusion(bf16[3072,384]{1,0:T(8,128)(2,1)S(1)} %bitcast.21, f32[2048,384]{1,0:T(8,128)} %fusion.29, bf16[2048,3072]{1,0:T(8,128)(2,1)} %bitcast.30, bf16[3072,384]{1,0:T(8,128)(2,1)} %bitcast.23), kind=kOutput, calls=%fused_computation.4 | convolution fusion | flops 9674686464 | bytes 33030144 | tf_op jit(solution)/shard_map/dot_general | solution.py:345
  225.7 0.7 copy-done.6
  226.4 0.8 iota_compare_fusion
  227.2 1.3 select_reduce_fusion
  228.5 0.6 copy.26
  229.2 27.3 %all-to-all-start = ((f32[2,2,4,128]{3,1,0,2:T(2,128)}), f32[2,2,4,128]{3,1,0,2:T(2,128)S(1)}, u32[]{:S(2)}, u32[]{:S(2)}) async-start(f32[2,2,4,128]{3,1,0,2:T(2,128)} %copy.26), calls=%async_computation.1 | async-start | bytes 16384 | tf_op jit(solution)/shard_map/all_to_all | solution.py:334
  256.5 5.6 %all-to-all-done = f32[2,2,4,128]{3,1,0,2:T(2,128)S(1)} async-done(((f32[2,2,4,128]{3,1,0,2:T(2,128)}), f32[2,2,4,128]{3,1,0,2:T(2,128)S(1)}, u32[]{:S(2)}, u32[]{:S(2)}) %all-to-all-start) | async-done | bytes 8224 | tf_op jit(solution)/shard_map/all_to_all | solution.py:334
  262.0 1.3 copy.28.weight
  263.4 3.6 reduce-scatter.2.cloned.1.call-done
  267.0 87.5 %give_back.1 = bf16[2,4,128,1536]{3,2,1,0:T(8,128)(2,1)} custom-call(bf16[2,2,4,128,1536]{4,3,2,1,0:T(8,128)(2,1)} %bitcast.18, f32[2,2,4,128,1]{4,3,2,1,0:T(8,128)} %copy.28.weight), custom_call_target="tpu_custom_call" | custom-call | tf_op jit(solution)/shard_map/give_back/pallas_call | solution.py:272
  354.6 7.0 %fusion.10 = bf16[1024,1536]{1,0:T(8,128)(2,1)} fusion(bf16[1024,1536]{1,0:T(8,128)(2,1)} %bitcast.20, s32[1024]{0:T(1024)S(1)} %fusion.23), kind=kOutput, calls=%fused_computation.14 | convolution fusion | flops 3223846912 | bytes 6295552 | tf_op jit(solution)/shard_map/dot_general | solution.py:354
  361.6 1.4 copy.34
  363.0 1.1 copy-done.2
  364.1 1.4 copy.35
  365.5 1.4 copy.36
  (21 shorter events, 0.1 us)
Async XLA Ops:
  7.2 259.9 %reduce-scatter.2.cloned.1.call-start = ((), (), s32[]{:S(2)}) async-start(), calls=%async_computation.2 | async-start | bytes 18874368 | tf_op jit(solution)/shard_map/reduce_scatter | solution.py:348
  9.0 4.3 %copy-start = (f32[8,192,384]{2,1,0:T(8,128)S(1)}, f32[8,192,384]{2,1,0:T(8,128)}, u32[]{:S(2)}) copy-start(f32[8,192,384]{2,1,0:T(8,128)} %param.12) | copy-start | bytes 7077892
  14.4 8.1 %copy-start.4 = (f32[8,192,384]{2,1,0:T(8,128)S(1)}, f32[8,192,384]{2,1,0:T(8,128)}, u32[]{:S(2)}) copy-start(f32[8,192,384]{2,1,0:T(8,128)} %param.11) | copy-start | bytes 7077892
  14.4 8.1 %copy-start.5 = (f32[8,192,384]{2,1,0:T(8,128)S(1)}, f32[8,192,384]{2,1,0:T(8,128)}, u32[]{:S(2)}) copy-start(f32[8,192,384]{2,1,0:T(8,128)} %param.10) | copy-start | bytes 7077892
  14.4 8.1 %copy-start.8 = (f32[192]{0:T(256)S(1)}, f32[192]{0:T(256)}, u32[]{:S(2)}) copy-start(f32[192]{0:T(256)} %param.9) | copy-start | bytes 2308
  194.1 11.6 %copy-start.1 = (bf16[2,8,192,384]{3,2,1,0:T(8,128)(2,1)S(1)}, bf16[2,8,192,384]{3,2,1,0:T(8,128)(2,1)}, u32[]{:S(2)}) copy-start(bf16[2,8,192,384]{3,2,1,0:T(8,128)(2,1)} %get-tuple-element.11) | copy-start | bytes 7077892
  225.7 0.7 copy-start.6
  225.7 0.7 copy-start.7
  229.2 32.9 %all-to-all-start = ((f32[2,2,4,128]{3,1,0,2:T(2,128)}), f32[2,2,4,128]{3,1,0,2:T(2,128)S(1)}, u32[]{:S(2)}, u32[]{:S(2)}) async-start(f32[2,2,4,128]{3,1,0,2:T(2,128)} %copy.26), calls=%async_computation.1 | async-start | bytes 16384 | tf_op jit(solution)/shard_map/all_to_all | solution.py:334
  354.6 7.0 %copy-start.3 = (bf16[2,8,192,384]{3,2,1,0:T(8,128)(2,1)S(1)}, bf16[2,8,192,384]{3,2,1,0:T(8,128)(2,1)}, u32[]{:S(2)}) copy-start(bf16[2,8,192,384]{3,2,1,0:T(8,128)(2,1)} %get-tuple-element.9) | copy-start | bytes 7077892
  361.6 2.5 copy-start.2
Sparse Core Ops, SparseCore 0:
  225.8 41.1 reduce-scatter.1
